TPU v7x, 32 devices: a whole 2x2x4 slice. The times are simulated.
32 devices in a mesh: fs: 8 (over z, y), tp: 4 (over x, core).
Axes of the slice: x: 2, y: 2, z: 4, core: 2. Of those that a mesh axis runs over, the one named last changes fastest.
Arguments:
- prompt_tokens: bfloat16 [768, 4096], P('tp'), may hold values from -6 to 6
- norm_gain: float32 [4096], P('fs'), may hold values from 0.1 to 1.9
- gate_trained: float32 [4096, 11264], P('fs', 'tp'), may hold values from -0.09375 to 0.09375
- up_trained: float32 [4096, 11264], P('fs', 'tp'), may hold values from -0.09375 to 0.09375
- down_trained: float32 [11264, 4096], P('fs', 'tp'), may hold values from -0.078125 to 0.078125
Outputs:
- gate_serving: bfloat16 [4096, 11264], P(None, 'fs')
- up_serving: bfloat16 [4096, 11264], P(None, 'fs')
- down_serving: bfloat16 [11264, 4096], P('fs')
- mixed: bfloat16 [768, 4096], P('tp', 'fs')
All inputs are finite; a program needn't handle non-finite values.
Results may differ from a plain program's by a relative error of at most 0.0082.
Values may be sent and summed in bfloat16 or wider, within the bound.
A program may use at most 128 MiB of HBM per device.

v0:
```python
import jax
import jax.numpy as jnp
from jax import lax
from jax.sharding import PartitionSpec as P


def on_device(prompt_tokens, norm_gain, gate_trained, up_trained, down_trained):
    fs_count = lax.axis_size("fs")
    gate_cast = (gate_trained * norm_gain[:, None]).astype(jnp.bfloat16)
    up_cast = (up_trained * norm_gain[:, None]).astype(jnp.bfloat16)
    down_cast = down_trained.astype(jnp.bfloat16)
    down_serving = lax.all_gather(down_cast, "tp", axis=1, tiled=True)
    gate_part, up_part = (
        lax.all_to_all(gate_cast, "tp", split_axis=0, concat_axis=1, tiled=True),
        lax.all_to_all(up_cast, "tp", split_axis=0, concat_axis=1, tiled=True),
    )
    gate_mid, up_mid = (
        lax.all_to_all(gate_part, "fs", split_axis=1, concat_axis=0, tiled=True),
        lax.all_to_all(up_part, "fs", split_axis=1, concat_axis=0, tiled=True),
    )
    share = gate_mid.shape[0] // fs_count
    width = gate_mid.shape[1]
    gate_blocks, up_blocks = (
        lax.all_gather(gate_mid.reshape(fs_count, share, width), "tp", axis=1, tiled=True),
        lax.all_gather(up_mid.reshape(fs_count, share, width), "tp", axis=1, tiled=True),
    )
    gate_serving = gate_blocks.reshape(-1, width)
    up_serving = up_blocks.reshape(-1, width)
    tokens = prompt_tokens.astype(jnp.float32)
    scale = lax.rsqrt(jnp.mean(tokens * tokens, axis=-1, keepdims=True) + 1e-06)
    normed = (tokens * scale).astype(jnp.bfloat16)
    contract = (((0,), (1,)), ((), ()))
    gate_cols = lax.dot_general(gate_serving, normed, contract, preferred_element_type=jnp.float32)
    up_cols = lax.dot_general(up_serving, normed, contract, preferred_element_type=jnp.float32)
    hidden_cols = (jax.nn.silu(gate_cols) * up_cols).astype(jnp.bfloat16)
    summed = lax.psum_scatter(
        lax.dot_general(
            down_serving, hidden_cols, (((0,), (0,)), ((), ())), preferred_element_type=jnp.float32
        ),
        "fs",
        scatter_dimension=0,
        tiled=True,
    )
    mixed = summed.T.astype(jnp.bfloat16)
    return (gate_serving, up_serving, down_serving, mixed)


def solution(mesh):
    return jax.shard_map(
        on_device,
        mesh=mesh,
        in_specs=(P("tp", None), P("fs"), P("fs", "tp"), P("fs", "tp"), P("fs", "tp")),
        out_specs=(P(None, "fs"), P(None, "fs"), P("fs", None), P("tp", "fs")),
        check_vma=False,
    )
```

profile of v0, /device:TPU:0, one launch (start us, length us, event | category | flops | bytes accessed | tf_op | source)
XLA Modules:
  0.0 524.6 jit_solution(6554279546055345411)
XLA Ops:
  7.2 0.0 all-gather.4.cloned.1.call-start
  7.2 5.5 %multiply_convert_fusion = (bf16[512,2816]{1,0:T(8,128)(2,1)S(1)}, bf16[512,2816]{1,0:T(8,128)(2,1)S(1)}) fusion(f32[512,2816]{1,0:T(8,128)} %param.8, f32[512]{0:T(512)} %param.6, f32[512,2816]{1,0:T(8,128)} %param.7), kind=kLoop, calls=%fused_computation | loop fusion | flops 5767168 | bytes 17303552 | tf_op jit(solution)/shard_map/convert_element_type | solution.py:10
  12.7 38.2 %all_to_all.64 = bf16[4,128,2816]{2,1,0:T(8,128)(2,1)} all-to-all(bf16[4,128,2816]{2,1,0:T(8,128)(2,1)S(1)} %bitcast.18), channel_id=1, replica_groups=mesh['fs'=8,'tp'=4] {'tp'}, dimensions={0} | all-to-all | bytes 5767168 | tf_op jit(solution)/shard_map/all_to_all | solution.py:14
  51.0 4.5 copy.9
  55.5 71.4 %all_to_all.65 = bf16[128,8,1408]{0,2,1:T(8,128)(2,1)} all-to-all(bf16[128,8,1408]{0,2,1:T(8,128)(2,1)} %bitcast.26), channel_id=1, replica_groups=mesh['fs'=8,'tp'=4] {'fs'}, dimensions={1} | all-to-all | bytes 5767168 | tf_op jit(solution)/shard_map/all_to_all | solution.py:18
  126.9 0.0 all-gather.4.cloned.1.call-update
  126.9 0.0 all-gather.6.cloned.1.call-start
  127.0 64.5 %all_to_all.66 = bf16[4,128,2816]{2,1,0:T(8,128)(2,1)} all-to-all(bf16[4,128,2816]{2,1,0:T(8,128)(2,1)S(1)} %bitcast.17), channel_id=1, replica_groups=mesh['fs'=8,'tp'=4] {'tp'}, dimensions={0} | all-to-all | bytes 5767168 | tf_op jit(solution)/shard_map/all_to_all | solution.py:15
  191.5 3.3 copy.11
  194.8 67.9 %all_to_all.67 = bf16[128,8,1408]{0,2,1:T(8,128)(2,1)} all-to-all(bf16[128,8,1408]{0,2,1:T(8,128)(2,1)S(1)} %bitcast.28), channel_id=1, replica_groups=mesh['fs'=8,'tp'=4] {'fs'}, dimensions={1} | all-to-all | bytes 5767168 | tf_op jit(solution)/shard_map/all_to_all | solution.py:19
  262.7 0.0 all-gather.6.cloned.1.call-update
  262.8 0.0 all-gather.8.cloned.1.call-start
  262.8 4.7 convert_element_type.26
  267.5 0.0 copy-start
  267.5 0.0 all-gather.8.cloned.1.call-update
  267.5 0.0 reduce-scatter.2.cloned.1.call-start
  267.6 1.6 copy-done
  269.1 0.4 fusion
  269.5 0.0 all-gather.4.cloned.1.call-done
  269.6 16.0 %copy.10 = bf16[8,512,1408]{2,1,0:T(8,128)(2,1)} copy(bf16[8,512,1408]{1,2,0:T(8,128)(2,1)} %all-gather.4.cloned.1.call-done) | data formatting | bytes 23068672 | tf_op jit(solution)/shard_map/all_gather | solution.py:24
  285.6 53.0 %all-gather.6.cloned.1.call-done = bf16[8,512,1408]{1,2,0:T(8,128)(2,1)} async-done(((bf16[8,128,1408]{1,2,0:T(8,128)(2,1)}), bf16[8,512,1408]{1,2,0:T(8,128)(2,1)}) %all-gather.6.cloned.1.call-update) | async-done | bytes 11534352 | tf_op jit(solution)/shard_map/all_gather | solution.py:25
  338.5 16.0 %copy.12 = bf16[8,512,1408]{2,1,0:T(8,128)(2,1)} copy(bf16[8,512,1408]{1,2,0:T(8,128)(2,1)} %all-gather.6.cloned.1.call-done) | data formatting | bytes 23068672 | tf_op jit(solution)/shard_map/all_gather | solution.py:25
  354.5 7.2 %fusion.3 = f32[1408,192]{0,1:T(8,128)S(1)} fusion(bf16[4096,1408]{1,0:T(8,128)(2,1)} %bitcast.19, bf16[192,4096]{1,0:T(8,128)(2,1)S(1)} %copy-done, f32[192]{0:T(256)S(1)} %add_rsqrt_fusion), kind=kOutput, calls=%fused_computation.9 | convolution fusion | flops 2216951808 | bytes 14189312 | tf_op jit(solution)/shard_map/dot_general | solution.py:33
  361.8 55.1 %all-gather.8.cloned.1.call-done = bf16[1408,4096]{1,0:T(8,128)(2,1)} async-done(((bf16[1408,1024]{1,0:T(8,128)(2,1)}), bf16[1408,4096]{1,0:T(8,128)(2,1)}) %all-gather.8.cloned.1.call-update) | async-done | bytes 11534352 | tf_op jit(solution)/shard_map/all_gather | solution.py:12
  416.8 14.4 %convolution_bitcast_fusion = f32[4096,192]{0,1:T(8,128)} fusion(bf16[1408,4096]{1,0:T(8,128)(2,1)} %all-gather.8.cloned.1.call-done, bf16[4096,1408]{1,0:T(8,128)(2,1)} %bitcast.21, f32[1408,192]{0,1:T(8,128)S(1)} %fusion.3, bf16[192,4096]{1,0:T(8,128)(2,1)S(1)} %copy-done, f32[192]{0:T(256)S(1)} %add_rsqrt_fusion), kind=kOutput, calls=%fused_computation.2 | convolution fusion | flops 4433166336 | bytes 28869376 | tf_op jit(solution)/shard_map/dot_general | solution.py:37
  431.3 0.0 reduce-scatter.2.cloned.1.call-update
  431.3 75.0 %reduce-scatter.2.cloned.1.call-done = f32[512,192]{0,1:T(8,128)} async-done(((f32[4096,192]{0,1:T(8,128)}), f32[512,192]{0,1:T(8,128)}) %reduce-scatter.2.cloned.1.call-update) | async-done | bytes 393232 | tf_op jit(solution)/shard_map/reduce_scatter | solution.py:36
  506.3 1.7 convert_bitcast_fusion
  508.0 10.1 %copy.14 = bf16[1408,4096]{1,0:T(8,128)(2,1)} copy(bf16[1408,4096]{1,0:T(8,128)(2,1)} %all-gather.8.cloned.1.call-done) | data formatting | bytes 23068672
  (1 shorter events, 0.0 us)
Async XLA Ops:
  7.2 262.4 %all-gather.4.cloned.1.call-start = ((), (), s32[]{:S(2)}) async-start(), calls=%async_computation.5 | async-start | bytes 14417920 | tf_op jit(solution)/shard_map/all_gather | solution.py:24
  126.9 211.6 %all-gather.6.cloned.1.call-start = ((), (), s32[]{:S(2)}) async-start(), calls=%async_computation.6 | async-start | bytes 14417920 | tf_op jit(solution)/shard_map/all_gather | solution.py:25
  262.8 154.1 %all-gather.8.cloned.1.call-start = ((), (), s32[]{:S(2)}) async-start(), calls=%async_computation.7 | async-start | bytes 14417920 | tf_op jit(solution)/shard_map/all_gather | solution.py:12
  267.5 1.6 copy-start
  267.5 238.8 %reduce-scatter.2.cloned.1.call-start = ((), (), s32[]{:S(2)}) async-start(), calls=%async_computation.8 | async-start | bytes 3538944 | tf_op jit(solution)/shard_map/reduce_scatter | solution.py:36
Sparse Core Ops, SparseCore 0:
  127.1 102.4 all-gather.3
  262.9 75.5 all-gather.5
  340.7 76.1 all-gather.7
  431.4 74.8 reduce-scatter.1
where the time goes:
time: 526 us; the launch traced here: 525 us
  blocking collectives  242 us (46%)
  waiting for transfers between devices  183 us (35%)
  local copies, waits for them, and re-layouts  51.5 us (10%)
  matrix products  21.7 us (4%)
  between operations  13.8 us (3%)
  other arithmetic  12.3 us (2%)
    reduce_scatter x1, waiting for transfers between devices, on_device(): lax.psum_scatter(lax.dot_general(down_serving, hidden_cols, (((0,), (0,))...  75 us
    all_to_all x1, blocking collectives, on_device(): lax.all_to_all(gate_part, 'fs', split_axis=1, concat_axis=0, tiled=True)  71.4 us
    all_to_all x1, blocking collectives, on_device(): lax.all_to_all(up_part, 'fs', split_axis=1, concat_axis=0, tiled=True)  67.9 us
    all_to_all x1, blocking collectives, on_device(): lax.all_to_all(up_cast, 'tp', split_axis=0, concat_axis=1, tiled=True)  64.5 us
    all_gather x1, waiting for transfers between devices, on_device(): down_serving = lax.all_gather(down_cast, 'tp', axis=1, tiled=True)  55.1 us
    all_gather x1, waiting for transfers between devices, on_device(): lax.all_gather(up_mid.reshape(fs_count, share, width), 'tp', axis=1, tile...  53 us
    all_to_all x1, blocking collectives, on_device(): lax.all_to_all(gate_cast, 'tp', split_axis=0, concat_axis=1, tiled=True)  38.2 us
    all_gather x1, local copies, waits for them, and re-layouts, on_device(): lax.all_gather(up_mid.reshape(fs_count, share, width), 'tp', axis=1, tile...  16 us
  transfers between devices with their start and end apart: 4, of which 3 were waited for; matrix products, arithmetic and copies ran while one was open for 9% of the time, Pallas kernels for 0%

commit v1 on v0

v1 whole, which is shorter than its diff:
```python
import functools

import jax
import jax.numpy as jnp
from jax import lax
from jax.experimental import pallas as pl
from jax.experimental.pallas import tpu as pltpu
from jax.sharding import PartitionSpec as P

MESH = pl.DeviceIdType.MESH
HOME, AWAY, BOTH = 0, 1, 2


def chunk_plan(rows):
    unit = 16
    side = max(unit, rows * 5 // 32 // unit * unit)
    left = rows - 2 * side
    first = left // 2 // unit * unit
    sizes = ((side, AWAY), (side, HOME), (first, BOTH), (left - first, BOTH))
    plan, at = [], 0
    for size, way in sizes:
        plan.append((at, size, way))
        at += size
    return tuple(plan)


def exchange_kernel(fs, tp, plan, w, d, out, dout, part, wbuf, dbuf,
                    part_send, part_recv, own_send, relay_send, land_recv,
                    sib_send, sib_recv, cross_send, down_send, down_recv, local_sem):
    f, t = lax.axis_index("fs"), lax.axis_index("tp")
    x, c = t // 2, lax.rem(t, 2)
    rows, width = w.shape[1], out.shape[2]
    dcols = d.shape[1]
    sib, far = 2 * x + 1 - c, 2 * (1 - x) + c
    chunks = len(plan)

    me = f * tp + t
    barrier = pltpu.get_barrier_semaphore()
    for i in range(1, fs * tp):
        other = lax.rem(me + i, fs * tp)
        pl.semaphore_signal(barrier, inc=1, device_id=(other // tp, lax.rem(other, tp)), device_id_type=MESH)
    pl.semaphore_wait(barrier, fs * tp - 1)

    half = fs // 2
    own_cross = (f // half) != x
    part_cross = (f // half) == x
    true = f >= 0

    def uses(cross, way, dropped):
        return jnp.logical_not(cross) if way == dropped else true

    def remote(src, dst, ssem, rsem, fs_to, tp_to):
        return pltpu.make_async_remote_copy(
            src_ref=src, dst_ref=dst, send_sem=ssem, recv_sem=rsem,
            device_id=(fs_to, tp_to), device_id_type=MESH)

    sent = []

    def send(cond, copy):
        @pl.when(cond)
        def _():
            copy.start()
        sent.append((cond, copy))

    def to_serve(src, sems, k, cond, home):
        at, size, _ = plan[k]
        for y in range(2):
            to = 2 * home + y
            for g in range(2):
                here = jnp.logical_and(to == f, c == g)
                send(jnp.logical_and(cond, jnp.logical_not(here)), remote(
                    src.at[g, pl.ds(at, size), pl.ds(y * width, width)],
                    out.at[g, pl.ds(f * rows + at, size), :],
                    sems.at[g, y, k], land_recv.at[f, k], to, 2 * x + g))

    def part_copy(g, k):
        at, size, _ = plan[k]
        return remote(w.at[g, pl.ds(at, size), :], part.at[g, pl.ds(at, size), :],
                      part_send.at[g, k], part_recv.at[g, k], f, far)

    for k in range(chunks):
        for g in range(2):
            send(uses(own_cross, plan[k][2], HOME), part_copy(g, k))
    for k in range(chunks):
        to_serve(w, own_send, k, uses(own_cross, plan[k][2], AWAY), t)
    block = pl.ds(pl.multiple_of(t * dcols, dcols), dcols)
    down_far = remote(d, dout.at[:, block], down_send.at[0], down_recv.at[0], f, far)
    down_sib = remote(d, dout.at[:, block], down_send.at[1], down_recv.at[1], f, sib)
    send(true, down_far)
    send(true, down_sib)
    take = pltpu.make_async_copy(d, dbuf, local_sem.at[0])
    take.start()
    take.wait()
    put_down = pltpu.make_async_copy(dbuf, dout.at[:, block], local_sem.at[0])
    put_down.start()

    for k in range(chunks):
        come = uses(part_cross, plan[k][2], HOME)

        @pl.when(come)
        def _():
            for g in range(2):
                part_copy(g, k).wait_recv()
        to_serve(part, relay_send, k, come, lax.rem(t + 2, tp))

    keeps = lax.rem(f // 2, 2) == c
    at_home = (f // half) == x
    cols = pl.ds(pl.multiple_of(lax.rem(f, 2) * width, width), width)
    mine = pl.ds(f * rows, rows)
    put = pltpu.make_async_copy(wbuf, out.at[c, mine, :], local_sem.at[1])

    @pl.when(keeps)
    def _():
        @pl.when(at_home)
        def _():
            get = pltpu.make_async_copy(w.at[c, :, cols], wbuf, local_sem.at[1])
            get.start()
            get.wait()

        @pl.when(jnp.logical_not(at_home))
        def _():
            get = pltpu.make_async_copy(part.at[c, :, cols], wbuf, local_sem.at[1])
            get.start()
            get.wait()
        put.start()
        put.wait()

    def landed(g, k, source):
        at, size, _ = plan[k]
        return out.at[g, pl.ds(source * rows + at, size), :]

    def down_on():
        remote(d, dout.at[:, block], down_send.at[0], down_recv.at[0], f, far).wait_recv()
        fblock = pl.ds(pl.multiple_of(far * dcols, dcols), dcols)
        send(true, remote(dout.at[:, fblock], dout.at[:, fblock], down_send.at[2], down_recv.at[2], f, sib))

    for k in range(chunks):
        way = plan[k][2]
        if k == chunks - 1:
            down_on()
        for i in range(fs):
            source = i
            ref = landed(c, k, source)
            kept = jnp.logical_and(keeps, f == source)
            fwd = remote(ref, ref, sib_send.at[source, k], sib_recv.at[source, k], f, sib)
            crossed = remote(ref, ref, cross_send.at[source, k], land_recv.at[source, k], f, far)

            @pl.when(jnp.logical_not(kept))
            def _():
                crossed.wait_recv()
            send(true, fwd)
            if way != BOTH:
                turn = (source // half) != (f // half)
                side = at_home if way == HOME else jnp.logical_not(at_home)
                send(jnp.logical_and(turn, side), crossed)

    for k in range(chunks):
        for source in range(fs):
            ref = landed(1 - c, k, source)
            remote(ref, ref, sib_send.at[source, k], sib_recv.at[source, k], f, sib).wait_recv()
    put_down.wait()
    down_sib.wait_recv()
    remote(dout.at[:, block], dout.at[:, block], down_send.at[2], down_recv.at[2], f, sib).wait_recv()
    for cond, copy in sent:
        @pl.when(cond)
        def _():
            copy.wait_send()


def exchange(w, d, fs, tp):
    rows, wide = w.shape[1:]
    width = wide * tp // fs
    plan = chunk_plan(rows)
    n = len(plan)
    dma = pltpu.SemaphoreType.DMA
    any_space = pl.BlockSpec(memory_space=pl.ANY)
    return pl.pallas_call(
        functools.partial(exchange_kernel, fs, tp, plan),
        out_shape=(
            jax.ShapeDtypeStruct((2, rows * fs, width), w.dtype),
            jax.ShapeDtypeStruct((d.shape[0], d.shape[1] * tp), d.dtype),
            jax.ShapeDtypeStruct(w.shape, w.dtype),
        ),
        in_specs=[any_space] * 2,
        out_specs=(any_space,) * 3,
        scratch_shapes=[
            pltpu.VMEM((rows, width), w.dtype),
            pltpu.VMEM(d.shape, d.dtype),
            dma((2, n)), dma((2, n)), dma((2, 2, n)), dma((2, 2, n)), dma((fs, n)),
            dma((fs, n)), dma((fs, n)), dma((fs, n)), dma((3,)), dma((3,)), dma((2,)),
        ],
        compiler_params=pltpu.CompilerParams(collective_id=0, has_side_effects=True),
    )(w, d)


def gather_by_kernel(gate_cast, up_cast, down_cast):
    both, down_serving, _ = exchange(
        jnp.stack([gate_cast, up_cast]), down_cast, lax.axis_size("fs"), lax.axis_size("tp"))
    return both[0], both[1], down_serving


def gather_by_collectives(gate_cast, up_cast, down_cast):
    fs_count = lax.axis_size("fs")
    down_serving = lax.all_gather(down_cast, "tp", axis=1, tiled=True)

    def serve(cast):
        part = lax.all_to_all(cast, "tp", split_axis=0, concat_axis=1, tiled=True)
        mid = lax.all_to_all(part, "fs", split_axis=1, concat_axis=0, tiled=True)
        share, width = mid.shape[0] // fs_count, mid.shape[1]
        blocks = lax.all_gather(mid.reshape(fs_count, share, width), "tp", axis=1, tiled=True)
        return blocks.reshape(-1, width)

    return serve(gate_cast), serve(up_cast), down_serving


def on_device(prompt_tokens, norm_gain, gate_trained, up_trained, down_trained):
    fs, tp = lax.axis_size("fs"), lax.axis_size("tp")
    gate_cast = (gate_trained * norm_gain[:, None]).astype(jnp.bfloat16)
    up_cast = (up_trained * norm_gain[:, None]).astype(jnp.bfloat16)
    down_cast = down_trained.astype(jnp.bfloat16)
    routed = fs == 2 * tp and tp == 4
    gather = gather_by_kernel if routed else gather_by_collectives
    gate_serving, up_serving, down_serving = gather(gate_cast, up_cast, down_cast)
    tokens = prompt_tokens.astype(jnp.float32)
    scale = lax.rsqrt(jnp.mean(tokens * tokens, axis=-1, keepdims=True) + 1e-06)
    normed = (tokens * scale).astype(jnp.bfloat16)
    contract = (((0,), (1,)), ((), ()))
    gate_cols = lax.dot_general(gate_serving, normed, contract, preferred_element_type=jnp.float32)
    up_cols = lax.dot_general(up_serving, normed, contract, preferred_element_type=jnp.float32)
    hidden_cols = (jax.nn.silu(gate_cols) * up_cols).astype(jnp.bfloat16)
    summed = lax.psum_scatter(
        lax.dot_general(
            down_serving, hidden_cols, (((0,), (0,)), ((), ())), preferred_element_type=jnp.float32
        ),
        "fs",
        scatter_dimension=0,
        tiled=True,
    )
    mixed = summed.T.astype(jnp.bfloat16)
    return (gate_serving, up_serving, down_serving, mixed)


def solution(mesh):
    return jax.shard_map(
        on_device,
        mesh=mesh,
        in_specs=(P("tp", None), P("fs"), P("fs", "tp"), P("fs", "tp"), P("fs", "tp")),
        out_specs=(P(None, "fs"), P(None, "fs"), P("fs", None), P("tp", "fs")),
        check_vma=False,
    )
```

time: 526 us -> 401 us (0.76)
  blocking collectives: 242 us -> 0 us
  Pallas kernels: 0 us -> 215 us
  waiting for transfers between devices: 183 us -> 116 us
  local copies, waits for them, and re-layouts: 51.5 us -> 24 us
    all_to_all x4 -> x0, blocking collectives: 242 us -> none  [the longest x1 71.4 us: on_device(): lax.all_to_all(gate_part, 'fs', split_axis=1, concat_axis=0, tiled=True)]
    pallas_call x0 -> x1, Pallas kernels: none -> 215 us  [exchange(): pl.pallas_call(functools.partial(exchange_kernel, fs, tp, plan), out_shap...]
    all_gather x3 -> x0, waiting for transfers between devices: 108 us -> none  [the longest x1 55.1 us: on_device(): down_serving = lax.all_gather(down_cast, 'tp', axis=1, tiled=True)]
    reduce_scatter x1, waiting for transfers between devices: 75 us -> 116 us  [on_device(): lax.psum_scatter(lax.dot_general(down_serving, hidden_cols, (((0,), (0,))...]
    all_gather x2 -> x0, local copies, waits for them, and re-layouts: 32 us -> none  [the longest x1 16 us: on_device(): lax.all_gather(up_mid.reshape(fs_count, share, width), 'tp', axis=1, tile...]
    squeeze x0 -> x1, local copies, waits for them, and re-layouts: none -> 12.6 us  [gather_by_kernel(): return (both[0], both[1], down_serving)]
    all_to_all x2 -> x0, local copies, waits for them, and re-layouts: 7.87 us -> none  [the longest x1 4.53 us: on_device(): lax.all_to_all(gate_cast, 'tp', split_axis=0, concat_axis=1, tiled=True)]
    another operation x0 -> x2, other arithmetic: none -> 6.93 us  [gather_by_kernel(): jnp.stack([gate_cast, up_cast])]
  transfers between devices with their start and end apart: 4 -> 1, of which waited for: 3 -> 1; matrix products, arithmetic and copies ran while one was open for 9% -> 0% of each run, Pallas kernels for 0% -> 0%
where the time goes in v1:
time: 401 us
  Pallas kernels  215 us (54%)
  waiting for transfers between devices  116 us (29%)
  local copies, waits for them, and re-layouts  24 us (6%)
  matrix products  17.2 us (4%)
  between operations  14.1 us (4%)
  other arithmetic  13.9 us (3%)
    pallas_call x1, Pallas kernels, exchange(): pl.pallas_call(functools.partial(exchange_kernel, fs, tp, plan), out_shap...  215 us
    reduce_scatter x1, waiting for transfers between devices, on_device(): lax.psum_scatter(lax.dot_general(down_serving, hidden_cols, (((0,), (0,))...  116 us
    dot_general x1, matrix products, on_device(): lax.dot_general(down_serving, hidden_cols, (((0,), (0,)), ((), ())), pref...  14.4 us
    squeeze x1, local copies, waits for them, and re-layouts, gather_by_kernel(): return (both[0], both[1], down_serving)  12.6 us
    unnamed x9, local copies, waits for them, and re-layouts  11.4 us
  transfers between devices with their start and end apart: 1, of which 1 were waited for; matrix products, arithmetic and copies ran while one was open for 0% of the time, Pallas kernels for 0%

profile of v1, /device:TPU:0, one launch (start us, length us, event | category | flops | bytes accessed | tf_op | source)
XLA Modules:
  0.0 400.6 jit_solution(14371075222030584280)
XLA Ops:
  7.2 0.0 copy-start.3
  7.2 0.0 reduce-scatter.2.cloned.1.call-start
  7.2 0.0 copy-start.1
  7.2 4.8 %convert_element_type.26.d = bf16[1408,1024]{1,0:T(8,128)(2,1)} convert(f32[1408,1024]{1,0:T(8,128)} %param.9) | non-fusion elementwise | flops 1441792 | bytes 8650752 | tf_op jit(solution)/shard_map/convert_element_type | solution.py:220
  12.1 0.0 copy-done.3
  12.1 0.0 copy-done.1
  12.1 3.9 fusion.2
  16.0 3.0 pad_maximum_fusion.w
  19.0 215.4 %shard_map.84 = (bf16[2,4096,1408]{2,1,0:T(8,128)(2,1)}, bf16[1408,4096]{1,0:T(8,128)(2,1)}, bf16[2,512,2816]{2,1,0:T(8,128)(2,1)}) custom-call(bf16[2,512,2816]{2,1,0:T(8,128)(2,1)} %pad_maximum_fusion.w, bf16[1408,1024]{1,0:T(8,128)(2,1)} %convert_element_type.26.d), custom_call_target="tpu_custom_call" | custom-call | tf_op jit(solution)/shard_map/pallas_call | solution.py:177
  234.4 0.0 copy-start.2
  234.4 12.6 %slice_bitcast_fusion = (bf16[4096,1408]{1,0:T(8,128)(2,1)}, bf16[4096,1408]{1,0:T(8,128)(2,1)S(1)}) fusion(bf16[2,4096,1408]{2,1,0:T(8,128)(2,1)} %get-tuple-element.6), kind=kLoop, calls=%fused_computation | loop fusion | bytes 46137344 | tf_op jit(solution)/shard_map/squeeze | solution.py:199
  247.1 0.0 copy-done.2
  247.1 0.0 copy-start
  247.1 0.4 fusion
  247.5 2.7 fusion.5
  250.3 1.3 copy-done
  251.5 14.4 %fusion.9 = f32[4096,192]{0,1:T(8,128)} fusion(bf16[1408,4096]{1,0:T(8,128)(2,1)} %get-tuple-element.18, bf16[4096,1408]{1,0:T(8,128)(2,1)} %get-tuple-element.17, f32[1408,192]{0,1:T(8,128)S(1)} %fusion.5, bf16[192,4096]{1,0:T(8,128)(2,1)S(1)} %copy-done.2, f32[192]{0:T(256)S(1)} %add_rsqrt_fusion), kind=kOutput, calls=%fused_computation.14 | convolution fusion | flops 4433166336 | bytes 28869376 | tf_op jit(solution)/shard_map/dot_general | solution.py:232
  266.0 0.0 reduce-scatter.2.cloned.1.call-update
  266.0 116.0 %reduce-scatter.2.cloned.1.call-done = f32[512,192]{0,1:T(8,128)} async-done(((f32[4096,192]{0,1:T(8,128)}), f32[512,192]{0,1:T(8,128)}) %reduce-scatter.2.cloned.1.call-update) | async-done | bytes 393232 | tf_op jit(solution)/shard_map/reduce_scatter | solution.py:231
  382.0 1.7 convert_bitcast_fusion
  383.7 10.1 %copy.10 = bf16[1408,4096]{1,0:T(8,128)(2,1)} copy(bf16[1408,4096]{1,0:T(8,128)(2,1)} %get-tuple-element.18) | data formatting | bytes 23068672
  (1 shorter events, 0.0 us)
Async XLA Ops:
  7.2 4.9 %copy-start.3 = (f32[512]{0:T(512)S(1)}, f32[512]{0:T(512)}, u32[]{:S(2)}) copy-start(f32[512]{0:T(512)} %param.6) | copy-start | bytes 6148
  7.2 374.8 %reduce-scatter.2.cloned.1.call-start = ((), (), s32[]{:S(2)}) async-start(), calls=%async_computation.1 | async-start | bytes 3538944 | tf_op jit(solution)/shard_map/reduce_scatter | solution.py:231
  7.2 4.8 %copy-start.1 = (f32[512,2816]{1,0:T(8,128)S(1)}, f32[512,2816]{1,0:T(8,128)}, u32[]{:S(2)}) copy-start(f32[512,2816]{1,0:T(8,128)} %param.7) | copy-start | bytes 17301508
  234.4 12.7 %copy-start.2 = (bf16[192,4096]{1,0:T(8,128)(2,1)S(1)}, bf16[192,4096]{1,0:T(8,128)(2,1)}, u32[]{:S(2)}) copy-start(bf16[192,4096]{1,0:T(8,128)(2,1)} %param.5) | copy-start | bytes 4718596
  247.1 4.4 %copy-start = (bf16[4096,1408]{1,0:T(8,128)(2,1)}, bf16[4096,1408]{1,0:T(8,128)(2,1)S(1)}, u32[]{:S(2)}) copy-start(bf16[4096,1408]{1,0:T(8,128)(2,1)S(1)} %get-tuple-element.16) | copy-start | bytes 34603012
Sparse Core Ops, SparseCore 0:
  266.1 115.8 reduce-scatter.1

commit v2 on v1

--- a/solution.py
+++ b/solution.py
@@ -24,12 +24,13 @@
     return tuple(plan)
 
 
-def exchange_kernel(fs, tp, plan, w, d, out, dout, part, wbuf, dbuf,
+def exchange_kernel(fs, tp, plan, wg, wu, d, out, dout, part, wbuf, dbuf,
                     part_send, part_recv, own_send, relay_send, land_recv,
                     sib_send, sib_recv, cross_send, down_send, down_recv, local_sem):
     f, t = lax.axis_index("fs"), lax.axis_index("tp")
     x, c = t // 2, lax.rem(t, 2)
-    rows, width = w.shape[1], out.shape[2]
+    w = (wg, wu)
+    rows, width = wg.shape[0], out.shape[2]
     dcols = d.shape[1]
     sib, far = 2 * x + 1 - c, 2 * (1 - x) + c
     chunks = len(plan)
@@ -62,27 +63,27 @@
             copy.start()
         sent.append((cond, copy))
 
-    def to_serve(src, sems, k, cond, home):
+    def to_serve(view, sems, k, cond, home):
         at, size, _ = plan[k]
         for y in range(2):
             to = 2 * home + y
             for g in range(2):
                 here = jnp.logical_and(to == f, c == g)
                 send(jnp.logical_and(cond, jnp.logical_not(here)), remote(
-                    src.at[g, pl.ds(at, size), pl.ds(y * width, width)],
+                    view(g, pl.ds(at, size), pl.ds(y * width, width)),
                     out.at[g, pl.ds(f * rows + at, size), :],
                     sems.at[g, y, k], land_recv.at[f, k], to, 2 * x + g))
 
     def part_copy(g, k):
         at, size, _ = plan[k]
-        return remote(w.at[g, pl.ds(at, size), :], part.at[g, pl.ds(at, size), :],
+        return remote(w[g].at[pl.ds(at, size), :], part.at[g, pl.ds(at, size), :],
                       part_send.at[g, k], part_recv.at[g, k], f, far)
 
     for k in range(chunks):
         for g in range(2):
             send(uses(own_cross, plan[k][2], HOME), part_copy(g, k))
     for k in range(chunks):
-        to_serve(w, own_send, k, uses(own_cross, plan[k][2], AWAY), t)
+        to_serve(lambda g, r, q: w[g].at[r, q], own_send, k, uses(own_cross, plan[k][2], AWAY), t)
     block = pl.ds(pl.multiple_of(t * dcols, dcols), dcols)
     down_far = remote(d, dout.at[:, block], down_send.at[0], down_recv.at[0], f, far)
     down_sib = remote(d, dout.at[:, block], down_send.at[1], down_recv.at[1], f, sib)
@@ -101,7 +102,7 @@
         def _():
             for g in range(2):
                 part_copy(g, k).wait_recv()
-        to_serve(part, relay_send, k, come, lax.rem(t + 2, tp))
+        to_serve(lambda g, r, q: part.at[g, r, q], relay_send, k, come, lax.rem(t + 2, tp))
 
     keeps = lax.rem(f // 2, 2) == c
     at_home = (f // half) == x
@@ -111,11 +112,12 @@
 
     @pl.when(keeps)
     def _():
-        @pl.when(at_home)
-        def _():
-            get = pltpu.make_async_copy(w.at[c, :, cols], wbuf, local_sem.at[1])
-            get.start()
-            get.wait()
+        for g in range(2):
+            @pl.when(jnp.logical_and(at_home, c == g))
+            def _():
+                get = pltpu.make_async_copy(w[g].at[:, cols], wbuf, local_sem.at[1])
+                get.start()
+                get.wait()
 
         @pl.when(jnp.logical_not(at_home))
         def _():
@@ -134,25 +136,40 @@
         fblock = pl.ds(pl.multiple_of(far * dcols, dcols), dcols)
         send(true, remote(dout.at[:, fblock], dout.at[:, fblock], down_send.at[2], down_recv.at[2], f, sib))
 
-    for k in range(chunks):
-        way = plan[k][2]
-        if k == chunks - 1:
+    def arrive(k, source, cond, cross):
+        ref = landed(c, k, source)
+        crossed = remote(ref, ref, cross_send.at[source, k], land_recv.at[source, k], f, far)
+        kept = jnp.logical_and(keeps, f == source)
+
+        @pl.when(jnp.logical_and(cond, jnp.logical_not(kept)))
+        def _():
+            crossed.wait_recv()
+        if cross:
+            send(cond, crossed)
+        send(cond, remote(ref, ref, sib_send.at[source, k], sib_recv.at[source, k], f, sib))
+
+    def turns(source):
+        return (source // half) != (f // half)
+
+    def side(k):
+        return at_home if plan[k][2] == HOME else jnp.logical_not(at_home)
+
+    one_way = [k for k in range(chunks) if plan[k][2] != BOTH]
+    both_ways = [k for k in range(chunks) if plan[k][2] == BOTH]
+    for k in one_way:
+        for source in range(fs):
+            arrive(k, source, jnp.logical_and(turns(source), side(k)), True)
+    for k in one_way:
+        for source in range(fs):
+            arrive(k, source, jnp.logical_not(turns(source)), False)
+    for k in both_ways:
+        if k == both_ways[-1]:
             down_on()
-        for i in range(fs):
-            source = i
-            ref = landed(c, k, source)
-            kept = jnp.logical_and(keeps, f == source)
-            fwd = remote(ref, ref, sib_send.at[source, k], sib_recv.at[source, k], f, sib)
-            crossed = remote(ref, ref, cross_send.at[source, k], land_recv.at[source, k], f, far)
-
-            @pl.when(jnp.logical_not(kept))
-            def _():
-                crossed.wait_recv()
-            send(true, fwd)
-            if way != BOTH:
-                turn = (source // half) != (f // half)
-                side = at_home if way == HOME else jnp.logical_not(at_home)
-                send(jnp.logical_and(turn, side), crossed)
+        for source in range(fs):
+            arrive(k, source, true, False)
+    for k in one_way:
+        for source in range(fs):
+            arrive(k, source, jnp.logical_and(turns(source), jnp.logical_not(side(k))), False)
 
     for k in range(chunks):
         for source in range(fs):
@@ -167,8 +184,8 @@
             copy.wait_send()
 
 
-def exchange(w, d, fs, tp):
-    rows, wide = w.shape[1:]
+def exchange(wg, wu, d, fs, tp):
+    rows, wide = wg.shape
     width = wide * tp // fs
     plan = chunk_plan(rows)
     n = len(plan)
@@ -177,26 +194,156 @@
     return pl.pallas_call(
         functools.partial(exchange_kernel, fs, tp, plan),
         out_shape=(
-            jax.ShapeDtypeStruct((2, rows * fs, width), w.dtype),
+            jax.ShapeDtypeStruct((2, rows * fs, width), wg.dtype),
             jax.ShapeDtypeStruct((d.shape[0], d.shape[1] * tp), d.dtype),
-            jax.ShapeDtypeStruct(w.shape, w.dtype),
-        ),
-        in_specs=[any_space] * 2,
+            jax.ShapeDtypeStruct((2, rows, wide), wg.dtype),
+        ),
+        in_specs=[any_space] * 3,
         out_specs=(any_space,) * 3,
         scratch_shapes=[
-            pltpu.VMEM((rows, width), w.dtype),
+            pltpu.VMEM((rows, width), wg.dtype),
             pltpu.VMEM(d.shape, d.dtype),
             dma((2, n)), dma((2, n)), dma((2, 2, n)), dma((2, 2, n)), dma((fs, n)),
             dma((fs, n)), dma((fs, n)), dma((fs, n)), dma((3,)), dma((3,)), dma((2,)),
         ],
         compiler_params=pltpu.CompilerParams(collective_id=0, has_side_effects=True),
-    )(w, d)
-
-
-def gather_by_kernel(gate_cast, up_cast, down_cast):
-    both, down_serving, _ = exchange(
-        jnp.stack([gate_cast, up_cast]), down_cast, lax.axis_size("fs"), lax.axis_size("tp"))
-    return both[0], both[1], down_serving
+    )(wg, wu, d)
+
+
+def hidden_kernel(tok, both, gate_out, up_out, hidden, acc, scale):
+    i = pl.program_id(0)
+    depth = gate_out.shape[0]
+
+    @pl.when(i == 0)
+    def _():
+        t = tok[...].astype(jnp.float32)
+        scale[...] = lax.rsqrt(jnp.mean(t * t, axis=-1, keepdims=True) + 1e-06)
+        acc[...] = jnp.zeros_like(acc)
+
+    gate_out[...] = both[0]
+    up_out[...] = both[1]
+    piece = tok[:, pl.ds(pl.multiple_of(i * depth, depth), depth)].astype(jnp.float32)
+    normed = (piece * scale[...]).astype(jnp.bfloat16)
+    for g in range(2):
+        acc[g] += jnp.dot(normed, both[g], preferred_element_type=jnp.float32)
+
+    @pl.when(i == pl.num_programs(0) - 1)
+    def _():
+        hidden[...] = (jax.nn.silu(acc[0]) * acc[1]).astype(hidden.dtype)
+
+
+def hidden_units(tok, both, steps):
+    _, features, width = both.shape
+    depth = features // steps
+    serving = jax.ShapeDtypeStruct((features, width), both.dtype)
+    return pl.pallas_call(
+        hidden_kernel,
+        grid=(steps,),
+        out_shape=(serving, serving, jax.ShapeDtypeStruct((tok.shape[0], width), both.dtype)),
+        in_specs=[
+            pl.BlockSpec(tok.shape, lambda i: (0, 0)),
+            pl.BlockSpec((2, depth, width), lambda i: (0, i, 0)),
+        ],
+        out_specs=(
+            pl.BlockSpec((depth, width), lambda i: (i, 0)),
+            pl.BlockSpec((depth, width), lambda i: (i, 0)),
+            pl.BlockSpec((tok.shape[0], width), lambda i: (0, 0)),
+        ),
+        scratch_shapes=[
+            pltpu.VMEM((2, tok.shape[0], width), jnp.float32),
+            pltpu.VMEM((tok.shape[0], 1), jnp.float32),
+        ],
+        compiler_params=pltpu.CompilerParams(dimension_semantics=("arbitrary",)),
+    )(tok, both)
+
+
+def partial_kernel(hidden, down, down_out, partial):
+    down_out[...] = down[...]
+    partial[0] = jnp.dot(hidden[...], down[...], preferred_element_type=jnp.float32).astype(partial.dtype)
+
+
+def partial_sums(hidden, down, blocks):
+    units, features = down.shape
+    width = features // blocks
+    return pl.pallas_call(
+        partial_kernel,
+        grid=(blocks,),
+        out_shape=(
+            jax.ShapeDtypeStruct(down.shape, down.dtype),
+            jax.ShapeDtypeStruct((blocks, hidden.shape[0], width), jnp.bfloat16),
+        ),
+        in_specs=[
+            pl.BlockSpec(hidden.shape, lambda j: (0, 0)),
+            pl.BlockSpec((units, width), lambda j: (0, j)),
+        ],
+        out_specs=(
+            pl.BlockSpec((units, width), lambda j: (0, j)),
+            pl.BlockSpec((1, hidden.shape[0], width), lambda j: (j, 0, 0)),
+        ),
+        compiler_params=pltpu.CompilerParams(dimension_semantics=("arbitrary",)),
+    )(hidden, down)
+
+
+def reduce_kernel(fs, p, mixed, ybuf, sbuf, zbuf, ysend, yrecv, zsend, zrecv):
+    f, t = lax.axis_index("fs"), lax.axis_index("tp")
+    z, y = f // 2, lax.rem(f, 2)
+    planes = fs // 2
+    barrier = pltpu.get_barrier_semaphore()
+    for i in range(1, fs):
+        pl.semaphore_signal(barrier, inc=1, device_id=(lax.rem(f + i, fs), t), device_id_type=MESH)
+    pl.semaphore_wait(barrier, fs - 1)
+
+    def remote(src, dst, ssem, rsem, to):
+        return pltpu.make_async_remote_copy(
+            src_ref=src, dst_ref=dst, send_sem=ssem, recv_sem=rsem,
+            device_id=(to, t), device_id_type=MESH)
+
+    order = sorted(range(1, planes), key=lambda o: abs(o - planes // 2)) + [0]
+    across, along = {}, {}
+    for off in order:
+        to = lax.rem(z + off, planes)
+        across[off] = remote(p.at[2 * to + 1 - y], ybuf.at[off], ysend.at[off], yrecv.at[off], 2 * z + 1 - y)
+        across[off].start()
+    for off in order:
+        to = lax.rem(z + off, planes)
+        across[off].wait_recv()
+        pair = p[2 * to + y].astype(jnp.float32) + ybuf[off].astype(jnp.float32)
+        if off:
+            sbuf[off] = pair.astype(sbuf.dtype)
+            along[off] = remote(sbuf.at[off], zbuf.at[off], zsend.at[off], zrecv.at[off], 2 * to + y)
+            along[off].start()
+        else:
+            total = pair
+    for off in order[:-1]:
+        along[off].wait_recv()
+        total += zbuf[off].astype(jnp.float32)
+    mixed[...] = total.astype(mixed.dtype)
+    for off in order:
+        across[off].wait_send()
+        if off:
+            along[off].wait_send()
+
+
+def reduce_over_fs(p, fs):
+    _, tokens, width = p.shape
+    dma = pltpu.SemaphoreType.DMA
+    slots = pltpu.VMEM((fs // 2, tokens, width), p.dtype)
+    return pl.pallas_call(
+        functools.partial(reduce_kernel, fs),
+        out_shape=jax.ShapeDtypeStruct((tokens, width), jnp.bfloat16),
+        in_specs=[pl.BlockSpec(memory_space=pltpu.VMEM)],
+        out_specs=pl.BlockSpec(memory_space=pltpu.VMEM),
+        scratch_shapes=[slots, slots, slots] + [dma((fs // 2,))] * 4,
+        compiler_params=pltpu.CompilerParams(collective_id=1, has_side_effects=True),
+    )(p)
+
+
+def by_kernels(prompt_tokens, gate_cast, up_cast, down_cast):
+    fs, tp = lax.axis_size("fs"), lax.axis_size("tp")
+    both, down_all, _ = exchange(gate_cast, up_cast, down_cast, fs, tp)
+    gate_serving, up_serving, hidden = hidden_units(prompt_tokens, both, fs)
+    down_serving, partial = partial_sums(hidden, down_all, fs)
+    return gate_serving, up_serving, down_serving, reduce_over_fs(partial, fs)
 
 
 def gather_by_collectives(gate_cast, up_cast, down_cast):
@@ -219,8 +366,9 @@
     up_cast = (up_trained * norm_gain[:, None]).astype(jnp.bfloat16)
     down_cast = down_trained.astype(jnp.bfloat16)
     routed = fs == 2 * tp and tp == 4
-    gather = gather_by_kernel if routed else gather_by_collectives
-    gate_serving, up_serving, down_serving = gather(gate_cast, up_cast, down_cast)
+    if routed:
+        return by_kernels(prompt_tokens, gate_cast, up_cast, down_cast)
+    gate_serving, up_serving, down_serving = gather_by_collectives(gate_cast, up_cast, down_cast)
     tokens = prompt_tokens.astype(jnp.float32)
     scale = lax.rsqrt(jnp.mean(tokens * tokens, axis=-1, keepdims=True) + 1e-06)
     normed = (tokens * scale).astype(jnp.bfloat16)

time: 401 us -> 335 us (0.84)
  waiting for transfers between devices: 116 us -> 0 us
  Pallas kernels: 215 us -> 321 us
  local copies, waits for them, and re-layouts: 24 us -> 1.63 us
  matrix products: 17.2 us -> 0 us
  between operations: 14.1 us -> 0.67 us
    reduce_scatter x1 -> x0, waiting for transfers between devices: 116 us -> none  [on_device(): lax.psum_scatter(lax.dot_general(down_serving, hidden_cols, (((0,), (0,))...]
    pallas_call x0 -> x3, Pallas kernels: none -> 107 us  [the longest x1 72.8 us: reduce_over_fs(): pl.pallas_call(functools.partial(reduce_kernel, fs), out_shape=jax.ShapeD...]
    dot_general x2 -> x0, matrix products: 17.2 us -> none  [the longest x1 14.4 us: on_device(): lax.dot_general(down_serving, hidden_cols, (((0,), (0,)), ((), ())), pref...]
    squeeze x1 -> x0, local copies, waits for them, and re-layouts: 12.6 us -> none  [gather_by_kernel(): return (both[0], both[1], down_serving)]
    unnamed x9 -> x5, local copies, waits for them, and re-layouts: 11.4 us -> 1.63 us
    another operation x2 -> x0, other arithmetic: 6.93 us -> none  [gather_by_kernel(): jnp.stack([gate_cast, up_cast])]
    convert_element_type x1, other arithmetic: 1.7 us -> 6.43 us  [on_device(): up_cast = (up_trained * norm_gain[:, None]).astype(jnp.bfloat16)]
  transfers between devices with their start and end apart: 1 -> 0, of which waited for: 1 -> 0; matrix products, arithmetic and copies ran while one was open for 0% -> 0% of each run, Pallas kernels for 0% -> 0%
where the time goes in v2:
time: 335 us; the launch traced here: 334 us
  Pallas kernels  321 us (96%)
  other arithmetic  11.3 us (3%)
    pallas_call x1, Pallas kernels, exchange(): pl.pallas_call(functools.partial(exchange_kernel, fs, tp, plan), out_shap...  214 us
    pallas_call x1, Pallas kernels, reduce_over_fs(): pl.pallas_call(functools.partial(reduce_kernel, fs), out_shape=jax.ShapeD...  72.8 us
    pallas_call x1, Pallas kernels, hidden_units(): pl.pallas_call(hidden_kernel, grid=(steps,), out_shape=(serving, serving,...  21.3 us
    pallas_call x1, Pallas kernels, partial_sums(): pl.pallas_call(partial_kernel, grid=(blocks,), out_shape=(jax.ShapeDtypeS...  12.6 us

profile of v2, /device:TPU:0, one launch (start us, length us, event | category | flops | bytes accessed | tf_op | source)
XLA Modules:
  0.0 334.5 jit_solution(3379464993840868141)
XLA Ops:
  0.6 0.0 copy-start
  0.6 0.0 copy-start.1
  0.7 4.8 %convert_element_type.11.d = bf16[1408,1024]{1,0:T(8,128)(2,1)} convert(f32[1408,1024]{1,0:T(8,128)} %param.9) | non-fusion elementwise | flops 1441792 | bytes 8650752 | tf_op jit(solution)/shard_map/convert_element_type | solution.py:367
  5.5 0.0 copy-done
  5.5 0.0 copy-done.1
  5.5 6.4 %multiply_convert_fusion = (bf16[512,2816]{1,0:T(8,128)(2,1)}, bf16[512,2816]{1,0:T(8,128)(2,1)}) fusion(f32[512,2816]{1,0:T(8,128)S(1)} %copy-done, f32[512]{0:T(512)S(1)} %copy-done.1, f32[512,2816]{1,0:T(8,128)} %param.7), kind=kLoop, calls=%fused_computation | loop fusion | flops 5767168 | bytes 17303552 | tf_op jit(solution)/shard_map/convert_element_type | solution.py:366
  11.9 214.2 %shard_map.84 = (bf16[2,4096,1408]{2,1,0:T(8,128)(2,1)}, bf16[1408,4096]{1,0:T(8,128)(2,1)}, bf16[2,512,2816]{2,1,0:T(8,128)(2,1)}) custom-call(bf16[512,2816]{1,0:T(8,128)(2,1)} %get-tuple-element.19.wg, bf16[512,2816]{1,0:T(8,128)(2,1)} %get-tuple-element.18.wu, bf16[1408,1024]{1,0:T(8,128)(2,1)} %convert_element_type.11.d), custom_call_target="tpu_custom_call" | custom-call | tf_op jit(solution)/shard_map/pallas_call | solution.py:194
  226.1 21.3 %shard_map.85 = (bf16[4096,1408]{1,0:T(8,128)(2,1)}, bf16[4096,1408]{1,0:T(8,128)(2,1)}, bf16[192,1408]{1,0:T(8,128)(2,1)}) custom-call(bf16[192,4096]{1,0:T(8,128)(2,1)} %tok.1, bf16[2,4096,1408]{2,1,0:T(8,128)(2,1)} %get-tuple-element.11.both), custom_call_target="tpu_custom_call" | custom-call | tf_op jit(solution)/shard_map/pallas_call | solution.py:239
  247.4 12.6 %shard_map.86 = (bf16[1408,4096]{1,0:T(8,128)(2,1)}, bf16[8,192,512]{2,1,0:T(8,128)(2,1)}) custom-call(bf16[192,1408]{1,0:T(8,128)(2,1)} %get-tuple-element.14.hidden, bf16[1408,4096]{1,0:T(8,128)(2,1)} %get-tuple-element.15.down), custom_call_target="tpu_custom_call" | custom-call | tf_op jit(solution)/shard_map/pallas_call | solution.py:268
  260.0 72.8 %shard_map.87 = bf16[192,512]{1,0:T(8,128)(2,1)} custom-call(bf16[8,192,512]{2,1,0:T(8,128)(2,1)} %get-tuple-element.17.p), custom_call_target="tpu_custom_call" | custom-call | tf_op jit(solution)/shard_map/pallas_call | solution.py:331
  332.8 1.6 copy.10
Async XLA Ops:
  0.6 4.9 %copy-start = (f32[512,2816]{1,0:T(8,128)S(1)}, f32[512,2816]{1,0:T(8,128)}, u32[]{:S(2)}) copy-start(f32[512,2816]{1,0:T(8,128)} %param.8) | copy-start | bytes 17301508
  0.6 4.8 %copy-start.1 = (f32[512]{0:T(512)S(1)}, f32[512]{0:T(512)}, u32[]{:S(2)}) copy-start(f32[512]{0:T(512)} %param.6) | copy-start | bytes 6148

commit v3 on v2

--- a/solution.py
+++ b/solution.py
@@ -11,14 +11,14 @@
 HOME, AWAY, BOTH = 0, 1, 2
 
 
+SHARES = ((1, AWAY), (2, BOTH), (4, AWAY), (7, HOME), (6, BOTH), (6, BOTH), (6, BOTH))
+
+
 def chunk_plan(rows):
-    unit = 16
-    side = max(unit, rows * 5 // 32 // unit * unit)
-    left = rows - 2 * side
-    first = left // 2 // unit * unit
-    sizes = ((side, AWAY), (side, HOME), (first, BOTH), (left - first, BOTH))
+    unit = max(16, rows // sum(share for share, _ in SHARES) // 16 * 16)
     plan, at = [], 0
-    for size, way in sizes:
+    for i, (share, way) in enumerate(SHARES):
+        size = rows - at if i == len(SHARES) - 1 else share * unit
         plan.append((at, size, way))
         at += size
     return tuple(plan)

time: 335 us -> 302 us (0.901)
  Pallas kernels: 321 us -> 287 us
    pallas_call x1, Pallas kernels: 72.8 us -> 30.4 us  [reduce_over_fs(): pl.pallas_call(functools.partial(reduce_kernel, fs), out_shape=jax.ShapeD...]
    pallas_call x1, Pallas kernels: 214 us -> 223 us  [exchange(): pl.pallas_call(functools.partial(exchange_kernel, fs, tp, plan), out_shap...]
where the time goes in v3:
time: 302 us; the launch traced here: 301 us
  Pallas kernels  287 us (95%)
  other arithmetic  11.3 us (4%)
    pallas_call x1, Pallas kernels, exchange(): pl.pallas_call(functools.partial(exchange_kernel, fs, tp, plan), out_shap...  223 us
    pallas_call x1, Pallas kernels, reduce_over_fs(): pl.pallas_call(functools.partial(reduce_kernel, fs), out_shape=jax.ShapeD...  30.4 us
    pallas_call x1, Pallas kernels, hidden_units(): pl.pallas_call(hidden_kernel, grid=(steps,), out_shape=(serving, serving,...  21.3 us
    pallas_call x1, Pallas kernels, partial_sums(): pl.pallas_call(partial_kernel, grid=(blocks,), out_shape=(jax.ShapeDtypeS...  12.6 us
    convert_element_type x1, other arithmetic, on_device(): up_cast = (up_trained * norm_gain[:, None]).astype(jnp.bfloat16)  6.43 us

profile of v3, /device:TPU:0, one launch (start us, length us, event | category | flops | bytes accessed | tf_op | source)
XLA Modules:
  0.0 301.0 jit_solution(13775465769781417125)
XLA Ops:
  0.6 0.0 copy-start
  0.6 0.0 copy-start.1
  0.7 4.8 %convert_element_type.11.d = bf16[1408,1024]{1,0:T(8,128)(2,1)} convert(f32[1408,1024]{1,0:T(8,128)} %param.9) | non-fusion elementwise | flops 1441792 | bytes 8650752 | tf_op jit(solution)/shard_map/convert_element_type | solution.py:367
  5.5 0.0 copy-done
  5.5 0.0 copy-done.1
  5.5 6.4 %multiply_convert_fusion = (bf16[512,2816]{1,0:T(8,128)(2,1)}, bf16[512,2816]{1,0:T(8,128)(2,1)}) fusion(f32[512,2816]{1,0:T(8,128)S(1)} %copy-done, f32[512]{0:T(512)S(1)} %copy-done.1, f32[512,2816]{1,0:T(8,128)} %param.7), kind=kLoop, calls=%fused_computation | loop fusion | flops 5767168 | bytes 17303552 | tf_op jit(solution)/shard_map/convert_element_type | solution.py:366
  11.9 223.1 %shard_map.84 = (bf16[2,4096,1408]{2,1,0:T(8,128)(2,1)}, bf16[1408,4096]{1,0:T(8,128)(2,1)}, bf16[2,512,2816]{2,1,0:T(8,128)(2,1)}) custom-call(bf16[512,2816]{1,0:T(8,128)(2,1)} %get-tuple-element.19.wg, bf16[512,2816]{1,0:T(8,128)(2,1)} %get-tuple-element.18.wu, bf16[1408,1024]{1,0:T(8,128)(2,1)} %convert_element_type.11.d), custom_call_target="tpu_custom_call" | custom-call | tf_op jit(solution)/shard_map/pallas_call | solution.py:194
  235.1 21.3 %shard_map.85 = (bf16[4096,1408]{1,0:T(8,128)(2,1)}, bf16[4096,1408]{1,0:T(8,128)(2,1)}, bf16[192,1408]{1,0:T(8,128)(2,1)}) custom-call(bf16[192,4096]{1,0:T(8,128)(2,1)} %tok.1, bf16[2,4096,1408]{2,1,0:T(8,128)(2,1)} %get-tuple-element.11.both), custom_call_target="tpu_custom_call" | custom-call | tf_op jit(solution)/shard_map/pallas_call | solution.py:239
  256.4 12.6 %shard_map.86 = (bf16[1408,4096]{1,0:T(8,128)(2,1)}, bf16[8,192,512]{2,1,0:T(8,128)(2,1)}) custom-call(bf16[192,1408]{1,0:T(8,128)(2,1)} %get-tuple-element.14.hidden, bf16[1408,4096]{1,0:T(8,128)(2,1)} %get-tuple-element.15.down), custom_call_target="tpu_custom_call" | custom-call | tf_op jit(solution)/shard_map/pallas_call | solution.py:268
  269.0 30.4 %shard_map.87 = bf16[192,512]{1,0:T(8,128)(2,1)} custom-call(bf16[8,192,512]{2,1,0:T(8,128)(2,1)} %get-tuple-element.17.p), custom_call_target="tpu_custom_call" | custom-call | tf_op jit(solution)/shard_map/pallas_call | solution.py:331
  299.4 1.6 copy.10
Async XLA Ops:
  0.6 4.9 %copy-start = (f32[512,2816]{1,0:T(8,128)S(1)}, f32[512,2816]{1,0:T(8,128)}, u32[]{:S(2)}) copy-start(f32[512,2816]{1,0:T(8,128)} %param.8) | copy-start | bytes 17301508
  0.6 4.8 %copy-start.1 = (f32[512]{0:T(512)S(1)}, f32[512]{0:T(512)}, u32[]{:S(2)}) copy-start(f32[512]{0:T(512)} %param.6) | copy-start | bytes 6148
